TPU v7x, 32 devices: a whole 2x2x4 slice. The times are simulated.
32 devices in a mesh: fs: 16 (over z, y, core), tp: 2 (over x).
Axes of the slice: x: 2, y: 2, z: 4, core: 2. Of those that a mesh axis runs over, the one named last changes fastest.
Arguments:
- tokens: bfloat16 [4096, 2048], P('fs'), may hold values from -6 to 6
- recurrent_input_gain: bfloat16 [2048], replicated, may hold values from 0.099609375 to 1.8984375
- recurrent_branch_weight: bfloat16 [2048, 1024], P('fs', 'tp'), may hold values from -0.125 to 0.125
- output_gate_weight: bfloat16 [2048, 1024], P('fs', 'tp'), may hold values from -0.125 to 0.125
- filter_taps: bfloat16 [4, 1024], P(None, 'tp'), may hold values from -3 to 3
- retention_gate_blocks: bfloat16 [2, 8, 128, 128], P(None, 'tp'), may hold values from -0.5 to 0.5
- input_gate_blocks: bfloat16 [2, 8, 128, 128], P(None, 'tp'), may hold values from -0.5 to 0.5
- channel_decay_rate: float32 [2, 1024], P(None, 'tp'), may hold values from 0 to 0.008, as said below
- position_log_decay: float32 [2, 4096, 1024], P(None, 'fs', 'tp'), may hold values from -0.7 to 0, as said below
- recurrent_output_weight: bfloat16 [1024, 2048], P('tp', 'fs'), may hold values from -0.1875 to 0.1875
- recurrent_output_gain: bfloat16 [2048], replicated, may hold values from 0.099609375 to 1.8984375
- feedforward_norm_gain: bfloat16 [2048], replicated, may hold values from 0.099609375 to 1.8984375
- feedforward_up_weight: bfloat16 [2048, 8192], P('fs', 'tp'), may hold values from -0.125 to 0.125
- feedforward_down_weight: bfloat16 [8192, 2048], P('tp', 'fs'), may hold values from -0.0625 to 0.0625
- feedforward_output_gain: bfloat16 [2048], replicated, may hold values from 0.099609375 to 1.8984375
Outputs:
- layer_out: bfloat16 [4096, 2048], P('fs')
Inputs may be any that keep to these rules, and one draw needn't show every extreme that they name: `channel_decay_rate`: positive rates, one for each channel and direction. `position_log_decay`: zero except at a few positions of each sequence and channel.
All inputs are finite; a program needn't handle non-finite values.
Results may differ from a plain program's by a relative error of at most 0.02.
Values may be sent and summed in bfloat16 or wider, within the bound.
A program may use at most 128 MiB of HBM per device.

v0:
```python
import jax
import jax.numpy as jnp
from jax import lax
from jax.sharding import PartitionSpec as P

EPS = 1e-06
GATE_STEEPNESS = 8.0


def root_norm(values, gain):
    return (
        values
        * lax.rsqrt(jnp.mean(values * values, axis=-1, keepdims=True) + EPS)
        * gain.astype(jnp.float32)
    )


def combine(earlier, later):
    return (earlier[0] * later[0], later[0] * earlier[1] + later[1])


def centred_conv(signal, taps):
    length = signal.shape[0]
    width_taps = taps.shape[0]
    left_pad = width_taps // 2
    padded = jnp.pad(signal.astype(jnp.float32), ((left_pad, width_taps - 1 - left_pad), (0, 0)))
    total = jnp.zeros(signal.shape, jnp.float32)
    for offset in range(width_taps):
        total = total + padded[offset : offset + length] * taps[offset].astype(jnp.float32)
    return total.astype(jnp.bfloat16)


def block_map(signal, matrices):
    block_width = matrices.shape[-1]
    shaped = signal.reshape(signal.shape[0], matrices.shape[0], block_width)
    mapped = jnp.einsum("tnc,ncd->tnd", shaped, matrices, preferred_element_type=jnp.float32)
    return mapped.reshape(signal.shape)


def linear_recurrence(
    convolved_output,
    retention_matrices,
    input_gate_matrices,
    decay_rate_row,
    decay_extra_block,
    reversed_scan,
):
    retention_gate = jax.nn.sigmoid(block_map(convolved_output, retention_matrices))
    admit = jax.nn.sigmoid(block_map(convolved_output, input_gate_matrices))
    logarithm_decay = -GATE_STEEPNESS * retention_gate * decay_rate_row[None, :] + decay_extra_block
    decay = jnp.exp(logarithm_decay)
    drive = jnp.sqrt(-jnp.expm1(2.0 * logarithm_decay)) * (
        admit * convolved_output.astype(jnp.float32)
    )
    _, state = lax.associative_scan(combine, (decay, drive), reverse=reversed_scan, axis=0)
    return state


def per_device(
    tokens,
    recurrent_input_gain,
    recurrent_branch_weight,
    output_gate_weight,
    filter_taps,
    retention_gate_blocks,
    input_gate_blocks,
    channel_decay_rate,
    position_log_decay,
    recurrent_output_weight,
    recurrent_output_gain,
    feedforward_norm_gain,
    feedforward_up_weight,
    feedforward_down_weight,
    feedforward_output_gain,
):
    normed = root_norm(tokens.astype(jnp.float32), recurrent_input_gain).astype(jnp.bfloat16)
    columns = normed
    recur_sum = jnp.dot(
        columns,
        lax.all_gather(recurrent_branch_weight, "fs", axis=0, tiled=True),
        preferred_element_type=jnp.float32,
    )
    gate_sum = jnp.dot(
        columns,
        lax.all_gather(output_gate_weight, "fs", axis=0, tiled=True),
        preferred_element_type=jnp.float32,
    )
    recur_in = recur_sum.astype(jnp.bfloat16)
    gate_in = lax.optimization_barrier(gate_sum.astype(jnp.bfloat16))
    convolved_output = lax.optimization_barrier(centred_conv(recur_in, filter_taps))
    forward_sweep = linear_recurrence(
        convolved_output,
        retention_gate_blocks[0],
        input_gate_blocks[0],
        channel_decay_rate[0],
        position_log_decay[0],
        False,
    )
    backward_sweep = linear_recurrence(
        convolved_output,
        retention_gate_blocks[1],
        input_gate_blocks[1],
        channel_decay_rate[1],
        position_log_decay[1],
        True,
    )
    hidden = ((forward_sweep + backward_sweep) * jax.nn.gelu(gate_in.astype(jnp.float32))).astype(
        jnp.bfloat16
    )
    mixer_cols = lax.all_gather(recurrent_output_weight, "fs", axis=1, tiled=True)
    partial_value = jnp.dot(hidden, mixer_cols, preferred_element_type=jnp.float32)
    mixed = lax.psum(partial_value.astype(jnp.bfloat16), "tp").astype(jnp.float32)
    stream = lax.optimization_barrier(
        (tokens.astype(jnp.float32) + root_norm(mixed, recurrent_output_gain)).astype(jnp.bfloat16)
    )
    normed_ff = root_norm(stream.astype(jnp.float32), feedforward_norm_gain).astype(jnp.bfloat16)
    columns = normed_ff
    lifted_sum = jnp.dot(
        columns,
        lax.all_gather(feedforward_up_weight, "fs", axis=0, tiled=True),
        preferred_element_type=jnp.float32,
    )
    lifted = jnp.square(jax.nn.relu(lifted_sum)).astype(jnp.bfloat16)
    down_cols = lax.all_gather(feedforward_down_weight, "fs", axis=1, tiled=True)
    lowered_part = jnp.dot(lifted, down_cols, preferred_element_type=jnp.float32)
    lowered = lax.psum(lowered_part.astype(jnp.bfloat16), "tp").astype(jnp.float32)
    return (stream.astype(jnp.float32) + root_norm(lowered, feedforward_output_gain)).astype(
        jnp.bfloat16
    )


def solution(mesh):
    in_specs = (
        P("fs", None),
        P(),
        P("fs", "tp"),
        P("fs", "tp"),
        P(None, "tp"),
        P(None, "tp", None, None),
        P(None, "tp", None, None),
        P(None, "tp"),
        P(None, "fs", "tp"),
        P("tp", "fs"),
        P(),
        P(),
        P("fs", "tp"),
        P("tp", "fs"),
        P(),
    )
    out_specs = P("fs", None)
    return jax.shard_map(
        per_device, mesh=mesh, in_specs=in_specs, out_specs=out_specs, check_vma=False
    )
```

profile of v0, /device:TPU:0, one launch (start us, length us, event | category | flops | bytes accessed | tf_op | source)
XLA Modules:
  0.0 505.1 jit_solution(16250297278894403998)
XLA Ops:
  6.5 0.7 all-gather.6.cloned.1.call-update
  7.3 0.7 all-gather.8.cloned.1.call-update
  8.8 0.8 slice_convert_fusion.3
  9.6 0.7 convert_element_type.80
  10.3 1.5 fusion.6
  11.9 0.8 slice_multiply_fusion.3
  12.6 41.1 %all-gather.6.cloned.1.call-done = bf16[2048,512]{1,0:T(8,128)(2,1)} async-done(((bf16[128,512]{1,0:T(8,128)(2,1)}), bf16[2048,512]{1,0:T(8,128)(2,1)}) %all-gather.6.cloned.1.call-update) | async-done | bytes 2097168 | tf_op jit(solution)/shard_map/all_gather | solution.py:80
  53.7 2.7 fusion.26
  58.7 1.0 copy.30
  59.7 1.0 copy.31
  60.7 2.4 fusion.60
  64.1 1.4 slice.448
  65.5 1.0 fusion.90
  90.4 0.7 pad_maximum_fusion.8
  91.2 0.8 fusion.74
  91.9 0.7 pad_maximum_fusion.6
  92.7 0.7 pad_maximum_fusion.4
  94.4 0.7 fusion.102
  96.6 0.9 add.357
  97.5 3.4 rev.2
  101.0 2.3 convolution_convert_fusion.2
  103.3 34.7 %all-gather.10.cloned.1.call-done = bf16[512,2048]{1,0:T(8,128)(2,1)} async-done(((bf16[512,128]{1,0:T(8,128)(2,1)}), bf16[512,2048]{1,0:T(8,128)(2,1)}) %all-gather.10.cloned.1.call-update) | async-done | bytes 2097168 | tf_op jit(solution)/shard_map/all_gather | solution.py:110
  138.0 3.4 convolution_convert_fusion.1
  142.9 37.9 %all-reduce.36.cloned.1.call-done = bf16[256,2048]{1,0:T(8,128)(2,1)} async-done(((bf16[256,2048]{1,0:T(8,128)(2,1)}), bf16[256,2048]{1,0:T(8,128)(2,1)}) %all-reduce.36.cloned.1.call-update) | async-done | bytes 1048592 | tf_op jit(solution)/shard_map/psum | solution.py:112
  180.8 1.5 fusion.2
  182.3 1.8 fusion.9
  184.4 124.9 %all-gather.12.cloned.1.call-done = bf16[2048,4096]{1,0:T(8,128)(2,1)} async-done(((bf16[128,4096]{1,0:T(8,128)(2,1)}), bf16[2048,4096]{1,0:T(8,128)(2,1)}) %all-gather.12.cloned.1.call-update) | async-done | bytes 16777232 | tf_op jit(solution)/shard_map/all_gather | solution.py:120
  309.3 130.1 %all-gather.14.cloned.1.call-done = bf16[4096,2048]{1,0:T(8,128)(2,1)} async-done(((bf16[4096,128]{1,0:T(8,128)(2,1)}), bf16[4096,2048]{1,0:T(8,128)(2,1)}) %all-gather.14.cloned.1.call-update) | async-done | bytes 16777232 | tf_op jit(solution)/shard_map/all_gather | solution.py:124
  439.4 16.2 %convolution_convert_fusion = bf16[256,2048]{1,0:T(8,128)(2,1)} fusion(bf16[4096,2048]{1,0:T(8,128)(2,1)} %all-gather.14.cloned.1.call-done, bf16[2048,4096]{1,0:T(8,128)(2,1)} %all-gather.12.cloned.1.call-done, bf16[256,2048]{1,0:T(8,128)(2,1)S(1)} %fusion.9, f32[2048]{0:T(1024)S(1)} %convert_element_type.94, f32[256]{0:T(256)S(1)} %add_rsqrt_fusion.1), kind=kOutput, calls=%fused_computation.13 | convolution fusion | flops 8595701760 | bytes 35660800 | tf_op jit(solution)/shard_map/dot_general | solution.py:125
  455.6 38.4 %all-reduce.38.cloned.1.call-done = bf16[256,2048]{1,0:T(8,128)(2,1)} async-done(((bf16[256,2048]{1,0:T(8,128)(2,1)}), bf16[256,2048]{1,0:T(8,128)(2,1)}) %all-reduce.38.cloned.1.call-update) | async-done | bytes 1048592 | tf_op jit(solution)/shard_map/psum | solution.py:126
  494.0 1.5 fusion.4
  495.6 2.6 fusion.13
  (283 shorter events, 31.2 us)
Async XLA Ops:
  6.5 47.2 %all-gather.6.cloned.1.call-start = ((), (), s32[]{:S(2)}) async-start(), calls=%async_computation | async-start | bytes 2228224 | tf_op jit(solution)/shard_map/all_gather | solution.py:80
  7.3 93.7 %all-gather.8.cloned.1.call-start = ((), (), s32[]{:S(2)}) async-start(), calls=%async_computation.1 | async-start | bytes 2228224 | tf_op jit(solution)/shard_map/all_gather | solution.py:85
  8.0 130.0 %all-gather.10.cloned.1.call-start = ((), (), s32[]{:S(2)}) async-start(), calls=%async_computation.2 | async-start | bytes 2228224 | tf_op jit(solution)/shard_map/all_gather | solution.py:110
  8.7 172.1 %all-reduce.36.cloned.1.call-start = ((), (), s32[]{:S(2)}) async-start(), calls=%async_computation.3 | async-start | bytes 2097152 | tf_op jit(solution)/shard_map/psum | solution.py:112
  10.3 46.1 %copy-start.28 = (f32[2048]{0:T(1024)}, f32[2048]{0:T(1024)S(1)}, u32[]{:S(2)}) copy-start(f32[2048]{0:T(1024)S(1)} %convert_element_type.80) | copy-start | bytes 24580
  11.9 44.5 %copy-start.35 = (f32[256]{0:T(256)}, f32[256]{0:T(256)S(1)}, u32[]{:S(2)}) copy-start(f32[256]{0:T(256)S(1)} %add_rsqrt_fusion.3) | copy-start | bytes 3076
  12.6 44.0 %copy-start.37 = (bf16[2,4,128,128]{3,2,1,0:T(8,128)(2,1)S(1)}, bf16[2,4,128,128]{3,2,1,0:T(8,128)(2,1)}, u32[]{:S(2)}) copy-start(bf16[2,4,128,128]{3,2,1,0:T(8,128)(2,1)} %param.20) | copy-start | bytes 786436
  79.0 11.3 %copy-start.15 = (f32[2,512]{1,0:T(2,128)S(1)}, f32[2,512]{1,0:T(2,128)}, u32[]{:S(2)}) copy-start(f32[2,512]{1,0:T(2,128)} %pad_add_fusion.1) | copy-start | bytes 12292
  79.0 11.3 %copy-start.30 = (f32[1,512]{1,0:T(1,128)S(1)}, f32[1,512]{1,0:T(1,128)}, u32[]{:S(2)}) copy-start(f32[1,512]{1,0:T(1,128)} %get-tuple-element.31) | copy-start | bytes 6148
  79.0 11.3 %copy-start.31 = (f32[1,512]{1,0:T(1,128)S(1)}, f32[1,512]{1,0:T(1,128)}, u32[]{:S(2)}) copy-start(f32[1,512]{1,0:T(1,128)} %get-tuple-element.32) | copy-start | bytes 6148
  79.0 11.3 %copy-start.10 = (f32[3,512]{1,0:T(4,128)S(1)}, f32[3,512]{1,0:T(4,128)}, u32[]{:S(2)}) copy-start(f32[3,512]{1,0:T(4,128)} %slice.473) | copy-start | bytes 18436
  79.0 11.3 %copy-start.11 = (f32[3,512]{1,0:T(4,128)S(1)}, f32[3,512]{1,0:T(4,128)}, u32[]{:S(2)}) copy-start(f32[3,512]{1,0:T(4,128)} %slice.490) | copy-start | bytes 18436
  79.0 11.3 %copy-start.25 = (f32[1,512]{1,0:T(1,128)S(1)}, f32[1,512]{1,0:T(1,128)}, u32[]{:S(2)}) copy-start(f32[1,512]{1,0:T(1,128)} %slice.575) | copy-start | bytes 6148
  79.0 11.4 %copy-start.4 = (f32[7,512]{1,0:T(8,128)S(1)}, f32[7,512]{1,0:T(8,128)}, u32[]{:S(2)}) copy-start(f32[7,512]{1,0:T(8,128)} %slice.492) | copy-start | bytes 43012
  79.1 12.1 %copy-start.1 = (f32[15,512]{1,0:T(8,128)S(1)}, f32[15,512]{1,0:T(8,128)}, u32[]{:S(2)}) copy-start(f32[15,512]{1,0:T(8,128)} %slice.461) | copy-start | bytes 92164
  79.5 8.9 %copy-start.7 = (f32[4,512]{1,0:T(4,128)}, f32[4,512]{1,0:T(4,128)S(1)}, u32[]{:S(2)}) copy-start(f32[4,512]{1,0:T(4,128)S(1)} %get-tuple-element.38) | copy-start | bytes 24580
  79.5 8.9 %copy-start.9 = (f32[4,512]{1,0:T(4,128)}, f32[4,512]{1,0:T(4,128)S(1)}, u32[]{:S(2)}) copy-start(f32[4,512]{1,0:T(4,128)S(1)} %get-tuple-element.37) | copy-start | bytes 24580
  88.4 5.1 %copy-start.21 = (f32[1,512]{1,0:T(1,128)S(1)}, f32[1,512]{1,0:T(1,128)}, u32[]{:S(2)}) copy-start(f32[1,512]{1,0:T(1,128)} %slice.571) | copy-start | bytes 6148
  93.7 1.6 copy-start.5
  93.7 1.6 copy-start.6
  93.8 1.6 copy-start.26
  93.8 1.6 copy-start.2
  93.8 1.6 copy-start.3
  93.8 1.6 copy-start.24
  93.9 1.7 copy-start.23
  96.5 4.5 copy-start
  96.5 4.5 copy-start.29
  96.5 4.5 copy-start.36
  141.5 167.8 %all-gather.12.cloned.1.call-start = ((), (), s32[]{:S(2)}) async-start(), calls=%async_computation.4 | async-start | bytes 17825792 | tf_op jit(solution)/shard_map/all_gather | solution.py:120
  142.0 297.3 %all-gather.14.cloned.1.call-start = ((), (), s32[]{:S(2)}) async-start(), calls=%async_computation.5 | async-start | bytes 17825792 | tf_op jit(solution)/shard_map/all_gather | solution.py:124
  142.6 351.4 %all-reduce.38.cloned.1.call-start = ((), (), s32[]{:S(2)}) async-start(), calls=%async_computation.6 | async-start | bytes 2097152 | tf_op jit(solution)/shard_map/psum | solution.py:126
  184.4 271.2 %copy-start.34 = (bf16[2048]{0:T(1024)(128)(2,1)S(1)}, bf16[2048]{0:T(1024)(128)(2,1)}, u32[]{:S(2)}) copy-start(bf16[2048]{0:T(1024)(128)(2,1)} %param.29) | copy-start | bytes 12292
  (14 other events, 14.6 us)
Sparse Core Ops, SparseCore 0:
  9.5 44.1 all-gather.5
  55.9 40.1 all-gather.7
  98.2 39.7 all-gather.9
  141.6 39.1 all-reduce.35
  182.8 126.4 all-gather.11
  311.3 128.0 all-gather.13
  455.7 38.2 all-reduce.37
where the time goes:
time: 506 us; the launch traced here: 505 us
  waiting for transfers between devices  410 us (81%)
  local copies, waits for them, and re-layouts  31.6 us (6%)
  matrix products  26 us (5%)
  other arithmetic  21.8 us (4%)
  between operations  14.9 us (3%)
    all_gather x1, waiting for transfers between devices, per_device(): lax.all_gather(feedforward_down_weight, 'fs', axis=1, tiled=True)  130 us
    all_gather x1, waiting for transfers between devices, per_device(): lax.all_gather(feedforward_up_weight, 'fs', axis=0, tiled=True)  125 us
    all_gather x1, waiting for transfers between devices, per_device(): lax.all_gather(recurrent_branch_weight, 'fs', axis=0, tiled=True)  41.1 us
    psum x1, waiting for transfers between devices, per_device(): lax.psum(lowered_part.astype(jnp.bfloat16), 'tp').astype(jnp.float32)  38.4 us
    psum x1, waiting for transfers between devices, per_device(): lax.psum(partial_value.astype(jnp.bfloat16), 'tp').astype(jnp.float32)  37.9 us
    all_gather x1, waiting for transfers between devices, per_device(): lax.all_gather(recurrent_output_weight, 'fs', axis=1, tiled=True)  34.7 us
    slice x98, local copies, waits for them, and re-layouts, linear_recurrence(): lax.associative_scan(combine, (decay, drive), reverse=reversed_scan, axis=0)  24.5 us
    dot_general x1, matrix products, per_device(): jnp.dot(lifted, down_cols, preferred_element_type=jnp.float32)  16.2 us
  transfers between devices with their start and end apart: 7, of which 6 were waited for; matrix products, arithmetic and copies ran while one was open for 11% of the time, Pallas kernels for 0%

commit v1 on v0

--- a/solution.py
+++ b/solution.py
@@ -1,6 +1,10 @@
+import functools
+
 import jax
 import jax.numpy as jnp
 from jax import lax
+from jax.experimental import pallas as pl
+from jax.experimental.pallas import tpu as pltpu
 from jax.sharding import PartitionSpec as P
 
 EPS = 1e-06
@@ -129,6 +133,426 @@
     )
 
 
+MESH = pl.DeviceIdType.MESH
+F32 = jnp.float32
+BF16 = jnp.bfloat16
+
+
+def shifted_rows(x, d, rows):
+    n = x.shape[0]
+    r = pltpu.roll(x, d % n, 0)
+    keep = rows >= d if d > 0 else rows < n + d
+    return jnp.where(keep, r, 0.0)
+
+
+def one_minus_exp(u):
+    poly = -u * (1.0 + u * (1 / 2) * (1.0 + u * (1 / 3) * (1.0 + u * (1 / 4) * (1.0 + u * (1 / 5)))))
+    return jnp.where(u > -0.1, poly, 1.0 - jnp.exp(u))
+
+
+def norm_rows(v, gain):
+    return v * lax.rsqrt(jnp.mean(v * v, axis=-1, keepdims=True) + EPS) * gain
+
+
+class Gather:
+    def __init__(self, buf, axis, sems, width):
+        self.buf, self.axis, self.width = buf, axis, width
+        self.recv, self.right, self.left, self.core, self.ysend = (sems.at[i] for i in range(5))
+
+    def at(self, slot):
+        part = pl.ds(pl.multiple_of(slot * self.width, self.width), self.width)
+        return self.buf.at[part, :] if self.axis == 0 else self.buf.at[:, part]
+
+    def copy(self, slot, sems, dev, src=None):
+        ref = self.at(slot)
+        return pltpu.make_async_remote_copy(
+            src_ref=ref if src is None else src,
+            dst_ref=ref,
+            send_sem=sems.at[slot],
+            recv_sem=self.recv.at[slot],
+            device_id=dev,
+            device_id_type=MESH,
+        )
+
+
+def mega_kernel(
+    nz,
+    x_ref, rg_in, out_in, up_in, dn_in, taps_ref, ret_ref, adm_ref, rate_ref, pld_ref,
+    g_in, g_rec, g_ff, g_out,
+    o_ref,
+    rg_buf, out_buf, up_buf, dn_buf, xn, rin, hid, part_s, part_r, stream, nff, lifted,
+    ys, yr, low, xs, xr,
+    rg_sem, out_sem, up_sem, dn_sem, loc_sem, mix_sem, nff_sem, ysem, xsem,
+):
+    f = lax.axis_index("fs")
+    t = lax.axis_index("tp")
+    z, y, c = f // 4, (f // 2) % 2, f % 2
+    rows_n, d_model = x_ref.shape
+    ff_q = up_buf.shape[1]
+
+    def dev(zz, yy, cc, tt=t):
+        return ((zz * 2 + yy) * 2 + cc, tt)
+
+    def slot_of(zz, yy, cc):
+        return (zz * 2 + yy) * 2 + cc
+
+    to_right, to_left = dev(z + 1, y, c), dev(z - 1, y, c)
+    to_y, to_c = dev(z, 1 - y, c), dev(z, y, 1 - c)
+    to_x = (f, 1 - t)
+    w = rg_in.shape[0]
+    RG = Gather(rg_buf, 0, rg_sem, w)
+    OUT = Gather(out_buf, 1, out_sem, w)
+    UP = Gather(up_buf, 0, up_sem, w)
+    DN = Gather(dn_buf, 1, dn_sem, w)
+    mine = pl.ds(pl.multiple_of(y * ff_q, ff_q), ff_q)
+    theirs = pl.ds(pl.multiple_of((1 - y) * ff_q, ff_q), ff_q)
+
+    locals_ = [
+        pltpu.make_async_copy(rg_in, RG.at(f), loc_sem.at[0]),
+        pltpu.make_async_copy(out_in, OUT.at(f), loc_sem.at[1]),
+        pltpu.make_async_copy(up_in.at[:, mine], UP.at(f), loc_sem.at[2]),
+        pltpu.make_async_copy(dn_in.at[mine, :], DN.at(f), loc_sem.at[3]),
+    ]
+    for cp in locals_:
+        cp.start()
+    up_y = UP.copy(f, UP.ysend, to_y, src=up_in.at[:, theirs])
+    dn_y = DN.copy(f, DN.ysend, to_y, src=dn_in.at[theirs, :])
+
+    def start(G, slot, sems, device, cond=None):
+        if cond is None:
+            G.copy(slot, sems, device).start()
+        else:
+            @pl.when(cond)
+            def _():
+                G.copy(slot, sems, device).start()
+
+    def wait_in(G, slot):
+        G.copy(slot, G.core, to_c).wait_recv()
+
+    def own(G, slot):
+        start(G, slot, G.right, to_right, z < nz - 1)
+        start(G, slot, G.left, to_left, z > 0)
+        start(G, slot, G.core, to_c)
+
+    def relay(G, r, sides):
+        for yy in sides:
+            @pl.when(z - r >= 0)
+            def _():
+                slot = slot_of(z - r, yy, c)
+                wait_in(G, slot)
+                start(G, slot, G.right, to_right, z < nz - 1)
+                start(G, slot, G.core, to_c)
+
+            @pl.when(z + r < nz)
+            def _():
+                slot = slot_of(z + r, yy, c)
+                wait_in(G, slot)
+                start(G, slot, G.left, to_left, z > 0)
+                start(G, slot, G.core, to_c)
+
+    def drain(G, sides):
+        for oz in range(nz):
+            for yy in sides:
+                slot = slot_of(oz, yy, c)
+
+                @pl.when((oz <= z) & (z < nz - 1))
+                def _():
+                    G.copy(slot, G.right, to_right).wait_send()
+
+                @pl.when((oz >= z) & (z > 0))
+                def _():
+                    G.copy(slot, G.left, to_left).wait_send()
+
+    def drain_core(G):
+        for oz in range(nz):
+            for yy in range(2):
+                G.copy(slot_of(oz, yy, c), G.core, to_c).wait_send()
+
+    locals_[0].wait()
+    own(RG, f)
+    locals_[1].wait()
+    own(OUT, f)
+    up_y.start()
+    dn_y.start()
+
+    chunk = 32
+
+    def norm_in(i, carry):
+        rs = pl.ds(pl.multiple_of(i * chunk, chunk), chunk)
+        xn[rs, :] = norm_rows(x_ref[rs, :].astype(F32), g_in[...]).astype(BF16)
+        return carry
+
+    lax.fori_loop(0, rows_n // chunk, norm_in, 0)
+
+    for G in (RG, OUT):
+        start(G, f, G.ysend, to_y)
+    for r in range(1, nz):
+        for G in (RG, OUT):
+            relay(G, r, [y])
+        if r == 1:
+            locals_[2].wait()
+            locals_[3].wait()
+            for G in (UP, DN):
+                own(G, f)
+        for G in (RG, OUT):
+            @pl.when(z - r >= 0)
+            def _():
+                start(G, slot_of(z - r, y, c), G.ysend, to_y)
+
+            @pl.when(z + r < nz)
+            def _():
+                start(G, slot_of(z + r, y, c), G.ysend, to_y)
+    fp = slot_of(z, 1 - y, c)
+    for G in (UP, DN):
+        wait_in(G, fp)
+        own(G, fp)
+    for G in (RG, OUT):
+        for oz in range(nz):
+            slot = slot_of(oz, 1 - y, c)
+            wait_in(G, slot)
+            start(G, slot, G.core, to_c)
+    for oz in range(nz):
+        for yy in range(2):
+            wait_in(RG, slot_of(oz, yy, 1 - c))
+
+    tile = 256
+
+    def project(i, carry):
+        cs = pl.ds(pl.multiple_of(i * tile, tile), tile)
+        rin[:, cs] = jnp.dot(xn[...], rg_buf[:, cs], preferred_element_type=F32).astype(BF16)
+        return carry
+
+    lax.fori_loop(0, rg_buf.shape[1] // tile, project, 0)
+
+    bw = ret_ref.shape[-1]
+    n_blk = ret_ref.shape[1]
+    width = n_blk * bw
+    rows = lax.broadcasted_iota(jnp.int32, (rows_n, bw), 0)
+    n_taps = taps_ref.shape[0]
+
+    def recur(j, carry):
+        cs = pl.ds(pl.multiple_of(j * bw, bw), bw)
+        gs = pl.ds(pl.multiple_of(width + j * bw, bw), bw)
+        sig = rin[:, cs].astype(F32)
+        total = jnp.zeros((rows_n, bw), F32)
+        for k in range(n_taps):
+            d = n_taps // 2 - k
+            s = sig if d == 0 else shifted_rows(sig, d, rows)
+            total = total + s * taps_ref[k : k + 1, cs]
+        conv = total.astype(BF16)
+        conv32 = conv.astype(F32)
+        both = jnp.zeros((rows_n, bw), F32)
+        for w_dir in range(2):
+            ret = jax.nn.sigmoid(jnp.dot(conv, ret_ref[w_dir, j], preferred_element_type=F32))
+            adm = jax.nn.sigmoid(jnp.dot(conv, adm_ref[w_dir, j], preferred_element_type=F32))
+            log_a = -GATE_STEEPNESS * ret * rate_ref[w_dir : w_dir + 1, cs] + pld_ref[w_dir, :, cs]
+            a = jnp.exp(log_a)
+            b = jnp.sqrt(one_minus_exp(2.0 * log_a)) * (adm * conv32)
+            d = 1
+            while d < rows_n:
+                sd = d if w_dir == 0 else -d
+                b = b + a * shifted_rows(b, sd, rows)
+                d *= 2
+                if d < rows_n:
+                    a = a * shifted_rows(a, sd, rows)
+            both = both + b
+        hid[:, cs] = (both * jax.nn.gelu(rin[:, gs].astype(F32))).astype(BF16)
+        return carry
+
+    lax.fori_loop(0, n_blk, recur, 0)
+
+    relay(UP, 1, [0, 1])
+    relay(DN, 1, [0, 1])
+    for oz in range(nz):
+        for yy in range(2):
+            wait_in(OUT, slot_of(oz, yy, 1 - c))
+
+    def mix(i, carry):
+        cs = pl.ds(pl.multiple_of(i * tile, tile), tile)
+        part_s[:, cs] = jnp.dot(hid[...], out_buf[:, cs], preferred_element_type=F32).astype(BF16)
+        return carry
+
+    lax.fori_loop(0, d_model // tile, mix, 0)
+    mix_cp = pltpu.make_async_remote_copy(
+        src_ref=part_s, dst_ref=part_r, send_sem=mix_sem.at[0], recv_sem=mix_sem.at[1],
+        device_id=to_x, device_id_type=MESH)
+    mix_cp.start()
+    mix_cp.wait_recv()
+    my_rows = pl.multiple_of(y * rows_n, rows_n)
+
+    def residual(i, carry):
+        rs = pl.ds(pl.multiple_of(i * chunk, chunk), chunk)
+        mixed = part_s[rs, :].astype(F32) + part_r[rs, :].astype(F32)
+        st = (x_ref[rs, :].astype(F32) + norm_rows(mixed, g_rec[...])).astype(BF16)
+        stream[rs, :] = st
+        ns = pl.ds(pl.multiple_of(my_rows + i * chunk, chunk), chunk)
+        nff[ns, :] = norm_rows(st.astype(F32), g_ff[...]).astype(BF16)
+        return carry
+
+    lax.fori_loop(0, rows_n // chunk, residual, 0)
+    my_nff = nff.at[pl.ds(my_rows, rows_n), :]
+    nff_cp = pltpu.make_async_remote_copy(
+        src_ref=my_nff, dst_ref=my_nff, send_sem=nff_sem.at[0], recv_sem=nff_sem.at[1],
+        device_id=to_y, device_id_type=MESH)
+    nff_cp.start()
+
+    relay(UP, 2, [0, 1])
+    relay(UP, 3, [0, 1])
+    nff_cp.wait_recv()
+    for oz in range(nz):
+        for yy in range(2):
+            wait_in(UP, slot_of(oz, yy, 1 - c))
+
+    def lift(i, carry):
+        cs = pl.ds(pl.multiple_of(i * tile, tile), tile)
+        v = jnp.dot(nff[...], up_buf[:, cs], preferred_element_type=F32)
+        lifted[:, cs] = jnp.square(jnp.maximum(v, 0.0)).astype(BF16)
+        return carry
+
+    piece = d_model // nz
+    their_rows = pl.multiple_of((1 - y) * rows_n, rows_n)
+    edge = (z == 0) | (z == nz - 1)
+
+    def piece_of(p):
+        near = (1, 0, 2, 3)[p]
+        base = jnp.where(edge, p, near)
+        return jnp.where(z < nz // 2, base, nz - 1 - base)
+
+    def cols_of(p):
+        return pl.ds(pl.multiple_of(piece_of(p) * piece, piece), piece)
+
+    def y_copy(p):
+        return pltpu.make_async_remote_copy(
+            src_ref=ys.at[p], dst_ref=yr.at[p], send_sem=ysem.at[0, p], recv_sem=ysem.at[1, p],
+            device_id=to_y, device_id_type=MESH)
+
+    def x_copy(p):
+        return pltpu.make_async_remote_copy(
+            src_ref=xs.at[p], dst_ref=xr.at[p], send_sem=xsem.at[0, p], recv_sem=xsem.at[1, p],
+            device_id=to_x, device_id_type=MESH)
+
+    def lower(p):
+        oz = piece_of(p)
+        for yy in range(2):
+            wait_in(DN, slot_of(oz, yy, 1 - c))
+        for s in range(piece // tile):
+            cs = pl.ds(pl.multiple_of(oz * piece + s * tile, tile), tile)
+            out_s = slice(s * tile, (s + 1) * tile)
+            ys[p, :, out_s] = jnp.dot(
+                lifted[pl.ds(their_rows, rows_n), :], dn_buf[:, cs], preferred_element_type=F32
+            ).astype(BF16)
+        y_copy(p).start()
+        for s in range(piece // tile):
+            cs = pl.ds(pl.multiple_of(oz * piece + s * tile, tile), tile)
+            low[p, :, s * tile : (s + 1) * tile] = jnp.dot(
+                lifted[pl.ds(my_rows, rows_n), :], dn_buf[:, cs], preferred_element_type=F32
+            )
+
+    def pass_on(p):
+        y_copy(p).wait_recv()
+        xs[p] = (low[p] + yr[p].astype(F32)).astype(BF16)
+        x_copy(p).start()
+
+    relay(DN, 2, [0, 1])
+    lax.fori_loop(0, ff_q // tile, lift, 0)
+    lower(0)
+    lower(1)
+    pass_on(0)
+    pass_on(1)
+    lower(2)
+    relay(DN, 3, [0, 1])
+    lower(3)
+    pass_on(2)
+    pass_on(3)
+    for p in range(nz):
+        x_copy(p).wait_recv()
+
+    def finish(i, carry):
+        rs = pl.ds(pl.multiple_of(i * chunk, chunk), chunk)
+        square = jnp.zeros((chunk, 1), F32)
+        for p in range(nz):
+            v = xs[p, rs, :].astype(F32) + xr[p, rs, :].astype(F32)
+            square = square + jnp.sum(v * v, axis=-1, keepdims=True)
+        scale = lax.rsqrt(square / d_model + EPS)
+        for p in range(nz):
+            cs = cols_of(p)
+            v = xs[p, rs, :].astype(F32) + xr[p, rs, :].astype(F32)
+            o_ref[rs, cs] = (stream[rs, cs].astype(F32) + v * scale * g_out[:, cs]).astype(BF16)
+        return carry
+
+    lax.fori_loop(0, rows_n // chunk, finish, 0)
+
+    mix_cp.wait_send()
+    nff_cp.wait_send()
+    up_y.wait_send()
+    dn_y.wait_send()
+    for G in (RG, OUT):
+        drain(G, [y])
+        drain_core(G)
+        for oz in range(nz):
+            G.copy(slot_of(oz, y, c), G.ysend, to_y).wait_send()
+    for G in (UP, DN):
+        drain(G, [0, 1])
+        drain_core(G)
+    for p in range(nz):
+        y_copy(p).wait_send()
+        x_copy(p).wait_send()
+
+
+def per_device_kernel(n_fs, *args):
+    (tokens, g_in, w_rec, w_gate, taps, ret, adm, rate, pld, w_out, g_rec, g_ff, w_up, w_dn, g_out) = args
+    nz = n_fs // 4
+    rows, d = tokens.shape
+    w_rg = jnp.concatenate([w_rec, w_gate], axis=1)
+    ff_q = w_up.shape[1] // 2
+    r_w = w_rec.shape[1]
+    vm = pl.BlockSpec(memory_space=pltpu.VMEM)
+    hb = pl.BlockSpec(memory_space=pl.ANY)
+    dma = pltpu.SemaphoreType.DMA
+
+    def gain(g):
+        return g.astype(F32).reshape(1, d)
+
+    return pl.pallas_call(
+        functools.partial(mega_kernel, nz),
+        out_shape=jax.ShapeDtypeStruct((rows, d), BF16),
+        in_specs=[vm, hb, hb, hb, hb] + [vm] * 9,
+        out_specs=vm,
+        scratch_shapes=[
+            pltpu.VMEM((d, 2 * r_w), BF16),
+            pltpu.VMEM((r_w, d), BF16),
+            pltpu.VMEM((d, ff_q), BF16),
+            pltpu.VMEM((ff_q, d), BF16),
+            pltpu.VMEM((rows, d), BF16),
+            pltpu.VMEM((rows, 2 * r_w), BF16),
+            pltpu.VMEM((rows, r_w), BF16),
+            pltpu.VMEM((rows, d), BF16),
+            pltpu.VMEM((rows, d), BF16),
+            pltpu.VMEM((rows, d), BF16),
+            pltpu.VMEM((2 * rows, d), BF16),
+            pltpu.VMEM((2 * rows, ff_q), BF16),
+            pltpu.VMEM((nz, rows, d // nz), BF16),
+            pltpu.VMEM((nz, rows, d // nz), BF16),
+            pltpu.VMEM((nz, rows, d // nz), F32),
+            pltpu.VMEM((nz, rows, d // nz), BF16),
+            pltpu.VMEM((nz, rows, d // nz), BF16),
+            dma((5, n_fs)),
+            dma((5, n_fs)),
+            dma((5, n_fs)),
+            dma((5, n_fs)),
+            dma((4,)),
+            dma((2,)),
+            dma((2,)),
+            dma((2, nz)),
+            dma((2, nz)),
+        ],
+        compiler_params=pltpu.CompilerParams(has_side_effects=True, vmem_limit_bytes=62 * 2**20),
+    )(
+        tokens, w_rg, w_out, w_up, w_dn, taps.astype(F32), ret, adm, rate, pld,
+        gain(g_in), gain(g_rec), gain(g_ff), gain(g_out),
+    )
+
+
 def solution(mesh):
     in_specs = (
         P("fs", None),
@@ -148,6 +572,8 @@
         P(),
     )
     out_specs = P("fs", None)
+    n_fs, n_tp = mesh.shape["fs"], mesh.shape["tp"]
+    body = functools.partial(per_device_kernel, n_fs) if (n_fs, n_tp) == (16, 2) else per_device
     return jax.shard_map(
-        per_device, mesh=mesh, in_specs=in_specs, out_specs=out_specs, check_vma=False
-    )
+        body, mesh=mesh, in_specs=in_specs, out_specs=out_specs, check_vma=False
+    )

time: 506 us -> 207 us (0.41)
  waiting for transfers between devices: 410 us -> 0 us
  Pallas kernels: 0 us -> 199 us
  local copies, waits for them, and re-layouts: 31.6 us -> 2.58 us
  matrix products: 26 us -> 0 us
  other arithmetic: 21.8 us -> 5.38 us
  between operations: 14.9 us -> 0.02 us
    all_gather x5 -> x0, waiting for transfers between devices: 331 us -> none  [the longest x1 130 us: per_device(): lax.all_gather(feedforward_down_weight, 'fs', axis=1, tiled=True)]
    pallas_call x0 -> x1, Pallas kernels: none -> 199 us  [per_device_kernel(): pl.pallas_call(functools.partial(mega_kernel, nz), out_shape=jax.ShapeDty...]
    psum x2 -> x0, waiting for transfers between devices: 76.3 us -> none  [the longest x1 38.4 us: per_device(): lax.psum(lowered_part.astype(jnp.bfloat16), 'tp').astype(jnp.float32)]
    dot_general x8 -> x0, matrix products: 26 us -> none  [the longest x1 16.2 us: per_device(): jnp.dot(lifted, down_cols, preferred_element_type=jnp.float32)]
    slice x98 -> x0, local copies, waits for them, and re-layouts: 24.5 us -> none  [linear_recurrence(): lax.associative_scan(combine, (decay, drive), reverse=reversed_scan, axis=0)]
  transfers between devices with their start and end apart: 7 -> 0, of which waited for: 6 -> 0; matrix products, arithmetic and copies ran while one was open for 11% -> 0% of each run, Pallas kernels for 0% -> 0%
where the time goes in v1:
time: 207 us
  Pallas kernels  199 us (96%)
  other arithmetic  5.38 us (3%)
  local copies, waits for them, and re-layouts  2.58 us (1%)
    pallas_call x1, Pallas kernels, per_device_kernel(): pl.pallas_call(functools.partial(mega_kernel, nz), out_shape=jax.ShapeDty...  199 us

profile of v1, /device:TPU:0, one launch (start us, length us, event | category | flops | bytes accessed | tf_op | source)
XLA Modules:
  0.0 206.5 jit_solution(11089780824195440211)
XLA Ops:
  0.0 0.0 copy-start
  0.0 1.3 reshape.28
  1.3 0.0 copy-done
  1.3 0.0 copy-start.1
  1.3 0.6 convert_element_type.2.taps_ref
  1.9 0.1 copy-done.1
  2.0 0.0 copy-start.2
  2.0 0.6 reshape.30
  2.6 0.1 copy-done.2
  2.7 0.0 copy-start.3
  2.7 0.6 reshape.32
  3.3 0.1 copy-done.3
  3.4 0.6 reshape.34
  4.0 1.7 pad_maximum_fusion.rg_in
  5.7 198.5 %shard_map.145 = bf16[256,2048]{1,0:T(8,128)(2,1)} custom-call(bf16[256,2048]{1,0:T(8,128)(2,1)} %x_ref.1, bf16[128,1024]{1,0:T(8,128)(2,1)} %pad_maximum_fusion.rg_in, bf16[512,128]{1,0:T(8,128)(2,1)} %out_in.1, bf16[128,4096]{1,0:T(8,128)(2,1)} %up_in.1, bf16[4096,128]{1,0:T(8,128)(2,1)} %dn_in.1, f32[4,512]{1,0:T(4,128)} %convert_element_type.2.taps_ref, ...), custom_call_target="tpu_custom_call" | custom-call | tf_op jit(solution)/shard_map/pallas_call | solution.py:516
  204.2 2.3 %copy.17 = bf16[256,2048]{1,0:T(8,128)(2,1)} copy(bf16[256,2048]{1,0:T(8,128)(2,1)} %shard_map.145) | data formatting | bytes 2097152
Async XLA Ops:
  0.0 1.3 copy-start
  1.3 0.7 copy-start.1
  2.0 0.7 copy-start.2
  2.7 0.7 copy-start.3

commit v2 on v1

--- a/solution.py
+++ b/solution.py
@@ -177,8 +177,8 @@
 
 def mega_kernel(
     nz,
-    x_ref, rg_in, out_in, up_in, dn_in, taps_ref, ret_ref, adm_ref, rate_ref, pld_ref,
-    g_in, g_rec, g_ff, g_out,
+    x_ref, rec_in, gate_in, out_in, up_in, dn_in, taps_ref, ret_ref, adm_ref, rate_ref, pld_ref,
+    gains,
     o_ref,
     rg_buf, out_buf, up_buf, dn_buf, xn, rin, hid, part_s, part_r, stream, nff, lifted,
     ys, yr, low, xs, xr,
@@ -199,7 +199,9 @@
     to_right, to_left = dev(z + 1, y, c), dev(z - 1, y, c)
     to_y, to_c = dev(z, 1 - y, c), dev(z, y, 1 - c)
     to_x = (f, 1 - t)
-    w = rg_in.shape[0]
+    w = rec_in.shape[0]
+    g_in, g_rec, g_ff, g_out = (gains.at[i : i + 1, :] for i in range(4))
+    half = rec_in.shape[1]
     RG = Gather(rg_buf, 0, rg_sem, w)
     OUT = Gather(out_buf, 1, out_sem, w)
     UP = Gather(up_buf, 0, up_sem, w)
@@ -208,10 +210,11 @@
     theirs = pl.ds(pl.multiple_of((1 - y) * ff_q, ff_q), ff_q)
 
     locals_ = [
-        pltpu.make_async_copy(rg_in, RG.at(f), loc_sem.at[0]),
+        pltpu.make_async_copy(rec_in, RG.at(f).at[:, :half], loc_sem.at[0]),
         pltpu.make_async_copy(out_in, OUT.at(f), loc_sem.at[1]),
         pltpu.make_async_copy(up_in.at[:, mine], UP.at(f), loc_sem.at[2]),
         pltpu.make_async_copy(dn_in.at[mine, :], DN.at(f), loc_sem.at[3]),
+        pltpu.make_async_copy(gate_in, RG.at(f).at[:, half:], loc_sem.at[4]),
     ]
     for cp in locals_:
         cp.start()
@@ -269,6 +272,7 @@
                 G.copy(slot_of(oz, yy, c), G.core, to_c).wait_send()
 
     locals_[0].wait()
+    locals_[4].wait()
     own(RG, f)
     locals_[1].wait()
     own(OUT, f)
@@ -291,9 +295,10 @@
             relay(G, r, [y])
         if r == 1:
             locals_[2].wait()
+            own(UP, f)
+        if r == 2:
             locals_[3].wait()
-            for G in (UP, DN):
-                own(G, f)
+            own(DN, f)
         for G in (RG, OUT):
             @pl.when(z - r >= 0)
             def _():
@@ -359,10 +364,11 @@
         hid[:, cs] = (both * jax.nn.gelu(rin[:, gs].astype(F32))).astype(BF16)
         return carry
 
+    relay(UP, 1, [y])
+    relay(DN, 1, [y])
     lax.fori_loop(0, n_blk, recur, 0)
-
-    relay(UP, 1, [0, 1])
-    relay(DN, 1, [0, 1])
+    relay(UP, 1, [1 - y])
+    relay(DN, 1, [1 - y])
     for oz in range(nz):
         for yy in range(2):
             wait_in(OUT, slot_of(oz, yy, 1 - c))
@@ -377,6 +383,8 @@
         src_ref=part_s, dst_ref=part_r, send_sem=mix_sem.at[0], recv_sem=mix_sem.at[1],
         device_id=to_x, device_id_type=MESH)
     mix_cp.start()
+    relay(UP, 2, [y])
+    relay(DN, 2, [y])
     mix_cp.wait_recv()
     my_rows = pl.multiple_of(y * rows_n, rows_n)
 
@@ -396,8 +404,9 @@
         device_id=to_y, device_id_type=MESH)
     nff_cp.start()
 
-    relay(UP, 2, [0, 1])
-    relay(UP, 3, [0, 1])
+    relay(UP, 2, [1 - y])
+    relay(DN, 2, [1 - y])
+    relay(UP, 3, [y, 1 - y])
     nff_cp.wait_recv()
     for oz in range(nz):
         for yy in range(2):
@@ -418,8 +427,11 @@
         base = jnp.where(edge, p, near)
         return jnp.where(z < nz // 2, base, nz - 1 - base)
 
-    def cols_of(p):
-        return pl.ds(pl.multiple_of(piece_of(p) * piece, piece), piece)
+    per = piece // tile
+
+    def cols_of(q):
+        start_at = piece_of(q // per) * piece + (q % per) * tile
+        return pl.ds(pl.multiple_of(start_at, tile), tile)
 
     def y_copy(p):
         return pltpu.make_async_remote_copy(
@@ -435,17 +447,18 @@
         oz = piece_of(p)
         for yy in range(2):
             wait_in(DN, slot_of(oz, yy, 1 - c))
-        for s in range(piece // tile):
-            cs = pl.ds(pl.multiple_of(oz * piece + s * tile, tile), tile)
-            out_s = slice(s * tile, (s + 1) * tile)
-            ys[p, :, out_s] = jnp.dot(
-                lifted[pl.ds(their_rows, rows_n), :], dn_buf[:, cs], preferred_element_type=F32
+        for q in range(p * per, (p + 1) * per):
+            ys[q] = jnp.dot(
+                lifted[pl.ds(their_rows, rows_n), :],
+                dn_buf[:, cols_of(q)],
+                preferred_element_type=F32,
             ).astype(BF16)
-        y_copy(p).start()
-        for s in range(piece // tile):
-            cs = pl.ds(pl.multiple_of(oz * piece + s * tile, tile), tile)
-            low[p, :, s * tile : (s + 1) * tile] = jnp.dot(
-                lifted[pl.ds(my_rows, rows_n), :], dn_buf[:, cs], preferred_element_type=F32
+            y_copy(q).start()
+        for q in range(p * per, (p + 1) * per):
+            low[q] = jnp.dot(
+                lifted[pl.ds(my_rows, rows_n), :],
+                dn_buf[:, cols_of(q)],
+                preferred_element_type=F32,
             )
 
     def pass_on(p):
@@ -453,28 +466,29 @@
         xs[p] = (low[p] + yr[p].astype(F32)).astype(BF16)
         x_copy(p).start()
 
-    relay(DN, 2, [0, 1])
     lax.fori_loop(0, ff_q // tile, lift, 0)
     lower(0)
     lower(1)
-    pass_on(0)
-    pass_on(1)
+    for q in range(2 * per):
+        pass_on(q)
     lower(2)
-    relay(DN, 3, [0, 1])
+    for q in range(2 * per, 3 * per):
+        pass_on(q)
+    relay(DN, 3, [y, 1 - y])
     lower(3)
-    pass_on(2)
-    pass_on(3)
-    for p in range(nz):
-        x_copy(p).wait_recv()
+    for q in range(3 * per, 4 * per):
+        pass_on(q)
+    for q in range(nz * per):
+        x_copy(q).wait_recv()
 
     def finish(i, carry):
         rs = pl.ds(pl.multiple_of(i * chunk, chunk), chunk)
         square = jnp.zeros((chunk, 1), F32)
-        for p in range(nz):
+        for p in range(nz * per):
             v = xs[p, rs, :].astype(F32) + xr[p, rs, :].astype(F32)
             square = square + jnp.sum(v * v, axis=-1, keepdims=True)
         scale = lax.rsqrt(square / d_model + EPS)
-        for p in range(nz):
+        for p in range(nz * per):
             cs = cols_of(p)
             v = xs[p, rs, :].astype(F32) + xr[p, rs, :].astype(F32)
             o_ref[rs, cs] = (stream[rs, cs].astype(F32) + v * scale * g_out[:, cs]).astype(BF16)
@@ -494,7 +508,7 @@
     for G in (UP, DN):
         drain(G, [0, 1])
         drain_core(G)
-    for p in range(nz):
+    for p in range(nz * per):
         y_copy(p).wait_send()
         x_copy(p).wait_send()
 
@@ -503,20 +517,19 @@
     (tokens, g_in, w_rec, w_gate, taps, ret, adm, rate, pld, w_out, g_rec, g_ff, w_up, w_dn, g_out) = args
     nz = n_fs // 4
     rows, d = tokens.shape
-    w_rg = jnp.concatenate([w_rec, w_gate], axis=1)
+    tile = 256
+    np_ = d // tile
+    gains = jnp.stack([g_in, g_rec, g_ff, g_out]).astype(F32)
     ff_q = w_up.shape[1] // 2
     r_w = w_rec.shape[1]
     vm = pl.BlockSpec(memory_space=pltpu.VMEM)
     hb = pl.BlockSpec(memory_space=pl.ANY)
     dma = pltpu.SemaphoreType.DMA
 
-    def gain(g):
-        return g.astype(F32).reshape(1, d)
-
     return pl.pallas_call(
         functools.partial(mega_kernel, nz),
         out_shape=jax.ShapeDtypeStruct((rows, d), BF16),
-        in_specs=[vm, hb, hb, hb, hb] + [vm] * 9,
+        in_specs=[vm, hb, hb, hb, hb, hb] + [vm] * 6,
         out_specs=vm,
         scratch_shapes=[
             pltpu.VMEM((d, 2 * r_w), BF16),
@@ -531,25 +544,24 @@
             pltpu.VMEM((rows, d), BF16),
             pltpu.VMEM((2 * rows, d), BF16),
             pltpu.VMEM((2 * rows, ff_q), BF16),
-            pltpu.VMEM((nz, rows, d // nz), BF16),
-            pltpu.VMEM((nz, rows, d // nz), BF16),
-            pltpu.VMEM((nz, rows, d // nz), F32),
-            pltpu.VMEM((nz, rows, d // nz), BF16),
-            pltpu.VMEM((nz, rows, d // nz), BF16),
+            pltpu.VMEM((np_, rows, tile), BF16),
+            pltpu.VMEM((np_, rows, tile), BF16),
+            pltpu.VMEM((np_, rows, tile), F32),
+            pltpu.VMEM((np_, rows, tile), BF16),
+            pltpu.VMEM((np_, rows, tile), BF16),
             dma((5, n_fs)),
             dma((5, n_fs)),
             dma((5, n_fs)),
             dma((5, n_fs)),
-            dma((4,)),
+            dma((5,)),
             dma((2,)),
             dma((2,)),
-            dma((2, nz)),
-            dma((2, nz)),
+            dma((2, np_)),
+            dma((2, np_)),
         ],
         compiler_params=pltpu.CompilerParams(has_side_effects=True, vmem_limit_bytes=62 * 2**20),
     )(
-        tokens, w_rg, w_out, w_up, w_dn, taps.astype(F32), ret, adm, rate, pld,
-        gain(g_in), gain(g_rec), gain(g_ff), gain(g_out),
+        tokens, w_rec, w_gate, w_out, w_up, w_dn, taps.astype(F32), ret, adm, rate, pld, gains,
     )
 
 

time: 207 us -> 218 us (1.053)
  Pallas kernels: 199 us -> 212 us
  other arithmetic: 5.38 us -> 1.27 us
    pallas_call x1, Pallas kernels: 199 us -> 212 us  [per_device_kernel(): pl.pallas_call(functools.partial(mega_kernel, nz), out_shape=jax.ShapeDty...]
    reshape x4 -> x0, other arithmetic: 3.08 us -> none  [gain(): return g.astype(F32).reshape(1, d)]
where the time goes in v2:
time: 218 us
  Pallas kernels  212 us (97%)
  local copies, waits for them, and re-layouts  4.46 us (2%)
    pallas_call x1, Pallas kernels, per_device_kernel(): pl.pallas_call(functools.partial(mega_kernel, nz), out_shape=jax.ShapeDty...  212 us

profile of v2, /device:TPU:0, one launch (start us, length us, event | category | flops | bytes accessed | tf_op | source)
XLA Modules:
  0.0 218.1 jit_solution(5758242741506818802)
XLA Ops:
  0.0 0.0 copy-start
  0.0 0.7 stack.15
  0.7 0.0 copy-done
  0.7 0.0 copy-start.1
  0.7 0.6 convert_element_type.6.taps_ref
  1.3 0.1 copy-done.1
  1.4 0.0 copy-start.2
  1.4 0.7 copy-done.2
  2.1 0.0 copy-start.3
  2.1 0.7 copy-done.3
  2.8 0.7 maximum_convert_fusion.gains
  3.4 212.4 %shard_map.145 = bf16[256,2048]{1,0:T(8,128)(2,1)} custom-call(bf16[256,2048]{1,0:T(8,128)(2,1)} %x_ref.1, bf16[128,512]{1,0:T(8,128)(2,1)} %rec_in.1, bf16[128,512]{1,0:T(8,128)(2,1)} %gate_in.1, bf16[512,128]{1,0:T(8,128)(2,1)} %out_in.1, bf16[128,4096]{1,0:T(8,128)(2,1)} %up_in.1, bf16[4096,128]{1,0:T(8,128)(2,1)} %dn_in.1, ...), custom_call_target="tpu_custom_call" | custom-call | tf_op jit(solution)/shard_map/pallas_call | solution.py:529
  215.8 2.3 %copy.17 = bf16[256,2048]{1,0:T(8,128)(2,1)} copy(bf16[256,2048]{1,0:T(8,128)(2,1)} %shard_map.145) | data formatting | bytes 2097152
  (3 shorter events, 0.0 us)
Async XLA Ops:
  0.0 0.7 copy-start
  0.7 0.7 copy-start.1
  1.4 0.7 copy-start.2
  2.1 0.7 copy-start.3
